TPU v7x, 32 devices: a whole 2x2x4 slice. The times are simulated.
32 devices in a mesh: ep: 8 (over z, x), tp: 4 (over y, core).
Axes of the slice: x: 2, y: 2, z: 4, core: 2. Of those that a mesh axis runs over, the one named last changes fastest.
Arguments:
- conv_value: bfloat16 [1024, 4096], P('tp', 'ep'), may hold values from -6 to 6
- conv_gate: bfloat16 [1024, 4096], P('tp', 'ep'), may hold values from -8 to 8
- conv_kernel: bfloat16 [31, 1024], P(None, 'tp'), may hold values from -1 to 1
- norm_gain: float32 [1024], replicated, may hold values from 0.1 to 1.9
- norm_shift: float32 [1024], replicated, may hold values from -3 to 3
- out_weight: bfloat16 [1024, 4096], P(None, 'tp'), may hold values from -0.1875 to 0.1875
- expert_input: bfloat16 [1024, 4096], P('ep'), may hold values from -6 to 6
- expert_ids: int32 [1024, 2], P('ep'), may hold values from 0 to 7, as said below
- pair_logits: float32 [1024, 2], P('ep'), may hold values from -6 to 6
- group_prob: float32 [1024], P('ep'), may hold values from 0.3 to 1
- expert_gate: bfloat16 [8, 4096, 2048], P('ep', None, 'tp'), may hold values from -0.09375 to 0.09375
- expert_up: bfloat16 [8, 4096, 2048], P('ep', None, 'tp'), may hold values from -0.09375 to 0.09375
- expert_down: bfloat16 [8, 2048, 4096], P('ep', None, 'tp'), may hold values from -0.125 to 0.125
Outputs:
- mixer_out: bfloat16 [4096, 4096], P('ep', 'tp')
- expert_out: bfloat16 [1024, 4096], P('ep', 'tp')
Inputs may be any that keep to these rules, and one draw needn't show every extreme that they name: `expert_ids`: the two experts of a token differ and lie in one group, ids g * 2 to (g + 1) * 2 - 1 for some g. The 128 tokens of one index of ep name every expert exactly 32 times.
All inputs are finite; a program needn't handle non-finite values.
Results may differ from a plain program's by a relative error of at most 0.0064.
Values may be sent and summed in bfloat16 or wider, within the bound.
A program may use at most 64 MiB of HBM per device.

v0:
```python
import jax
import jax.numpy as jnp
from jax import lax
from jax.sharding import PartitionSpec as P


def extended(cells, sides, width):
    for axis, dim in sides:
        count = lax.axis_size(axis)
        ends = count - 1
        head = lax.slice_in_dim(cells, 0, width, axis=dim)
        tail = lax.slice_in_dim(cells, cells.shape[dim] - width, cells.shape[dim], axis=dim)
        cells = jnp.concatenate(
            [
                lax.ppermute(tail, axis, [(i, (i + 1) % count) for i in range(ends)]),
                cells,
                lax.ppermute(head, axis, [((i + 1) % count, i) for i in range(ends)]),
            ],
            axis=dim,
        )
    return cells


def norm_swish(conv_out, norm_gain, norm_shift):
    values = conv_out.astype(jnp.float32)
    center = jnp.mean(values, axis=0, keepdims=True)
    spread = jnp.mean(jnp.square(values - center), axis=0, keepdims=True)
    normed = (values - center) * lax.rsqrt(spread + 1e-05) * norm_gain[:, None] + norm_shift[
        :, None
    ]
    return jax.nn.silu(normed).astype(jnp.bfloat16)


def route_weights(pair_logits, group_prob):
    share = jax.nn.sigmoid(pair_logits[:, 0] - pair_logits[:, 1])
    return jnp.stack([share, 1.0 - share], axis=1) * group_prob[:, None]


def local(
    conv_value,
    conv_gate,
    conv_kernel,
    norm_gain,
    norm_shift,
    out_weight,
    expert_input,
    expert_ids,
    pair_logits,
    group_prob,
    expert_gate,
    expert_up,
    expert_down,
):
    gated = (conv_value.astype(jnp.float32) * jax.nn.sigmoid(conv_gate.astype(jnp.float32))).astype(
        jnp.bfloat16
    )
    taps = conv_kernel.shape[0]
    reach = (taps - 1) // 2
    length = gated.shape[1]
    padded = extended(gated, (("ep", 1),), reach).astype(jnp.float32)
    kernel_f = conv_kernel.astype(jnp.float32)
    summed = jnp.zeros(gated.shape, jnp.float32)
    for offset in range(taps):
        summed = summed + kernel_f[offset][:, None] * padded[:, offset : offset + length]
    conv_out = summed.astype(jnp.bfloat16)
    experts = lax.axis_size("ep")
    flat = expert_ids.reshape(-1)
    onehot = (flat[:, None] == jnp.arange(experts, dtype=jnp.int32)[None, :]).astype(jnp.int32)
    before = jnp.cumsum(onehot, axis=0) - onehot
    slots = flat.shape[0] // experts
    position = flat * slots + jnp.sum(before * onehot, axis=1)
    source_row = (
        jnp.zeros_like(flat).at[position].set(jnp.arange(flat.shape[0], dtype=jnp.int32) // 2)
    )
    slice_width = expert_input.shape[1] // lax.axis_size("tp")
    columns = lax.dynamic_slice_in_dim(
        expert_input, lax.axis_index("tp") * slice_width, slice_width, 1
    )
    sliced = lax.all_to_all(columns[source_row], "ep", split_axis=0, concat_axis=0, tiled=True)
    arrived = lax.all_gather(sliced, "tp", axis=1, tiled=True)
    gate_val = jnp.dot(arrived, expert_gate[0], preferred_element_type=jnp.float32)
    up_val = jnp.dot(arrived, expert_up[0], preferred_element_type=jnp.float32)
    hidden = (jax.nn.silu(gate_val) * up_val).astype(jnp.bfloat16)
    down_local = expert_down[0]
    whole_conv = lax.all_gather(conv_out, "tp", axis=0, tiled=True)
    produced = jnp.dot(
        lax.all_gather(hidden, "tp", axis=1, tiled=True),
        down_local,
        preferred_element_type=jnp.float32,
    )
    returned = lax.all_to_all(
        produced.astype(jnp.bfloat16), "ep", split_axis=0, concat_axis=0, tiled=True
    )
    copies = returned[position].reshape(-1, 2, returned.shape[1]).astype(jnp.float32)
    weights = route_weights(pair_logits, group_prob)
    expert_out = jnp.sum(copies * weights[:, :, None], axis=1).astype(jnp.bfloat16)
    swished = norm_swish(whole_conv, norm_gain, norm_shift)
    mixer_out = lax.dot_general(
        swished, out_weight, (((0,), (0,)), ((), ())), preferred_element_type=jnp.float32
    ).astype(jnp.bfloat16)
    return (mixer_out, expert_out)


def solution(mesh):
    placed = (
        P("tp", "ep"),
        P("tp", "ep"),
        P(None, "tp"),
        P(),
        P(),
        P(None, "tp"),
        P("ep", None),
        P("ep", None),
        P("ep", None),
        P("ep"),
        P("ep", None, "tp"),
        P("ep", None, "tp"),
        P("ep", None, "tp"),
    )
    return jax.shard_map(
        local, mesh=mesh, in_specs=placed, out_specs=(P("ep", "tp"), P("ep", "tp")), check_vma=False
    )
```

profile of v0, /device:TPU:0, one launch (start us, length us, event | category | flops | bytes accessed | tf_op | source)
XLA Modules:
  0.0 132.5 jit_solution(13221667714410527884)
XLA Ops:
  7.2 0.0 copy-start
  7.2 0.0 all-gather.6.cloned.1.call-start
  7.2 0.9 copy.17
  8.2 0.1 eq.29
  8.3 0.1 eq.25
  8.4 0.7 broadcast_multiply_fusion.1
  9.1 0.6 reduce-window.6
  9.7 0.2 slice_reduce_fusion
  10.0 0.1 copy.16
  10.1 0.1 mul.484
  10.2 0.1 fusion.64
  10.3 1.4 %scatter_custom_fusion = s32[256]{0:T(256)S(1)} fusion(s32[256]{0:T(256)S(1)} %bitcast.98, s32[256]{0:T(256)S(1)} %and_select_fusion, s32[]{:T(128)} %constant.42.clone.1), kind=kCustom, calls=%fused_computation.116 | custom fusion | bytes 1028 | tf_op jit(solution)/shard_map/scatter | solution.py:73
  11.8 1.0 constant_dynamic-slice_fusion
  12.7 0.0 copy-start.1
  12.7 0.0 copy-start.2
  12.8 1.2 gather_fusion
  13.9 0.0 copy-start.3
  13.9 21.7 %all_to_all.24 = bf16[8,32,1024]{2,1,0:T(8,128)(2,1)} all-to-all(bf16[8,32,1024]{2,1,0:T(8,128)(2,1)S(1)} %bitcast.65), channel_id=1, replica_groups=mesh['ep'=8,'tp'=4] {'ep'}, dimensions={0} | all-to-all | bytes 1048576 | tf_op jit(solution)/shard_map/all_to_all | solution.py:79
  35.7 0.0 all-gather.6.cloned.1.call-update
  35.7 0.0 all-gather.4.cloned.1.call-start
  35.7 0.0 copy-done.1
  35.7 0.0 copy-done.2
  35.7 0.1 multiply_convert_fusion
  35.9 0.1 fusion.69
  36.0 3.3 %collective-permute-start = (bf16[256,15]{1,0:T(8,128)(2,1)S(1)}, bf16[256,15]{1,0:T(8,128)(2,1)S(1)}, u32[]{:S(2)}, u32[]{:S(2)}) collective-permute-start(bf16[256,15]{1,0:T(8,128)(2,1)S(1)} %get-tuple-element.4), channel_id=1, source_target_pairs={{0,4},{4,8},{8,12},{12,16},{16,20},{20,24},{24,28},{1,5},{5,9},{9,... | collective-permute-start | bytes 23048 | tf_op jit(solution)/shard_map/ppermute | solution.py:15
  39.3 1.3 collective-permute-start.1
  40.6 0.0 copy-done.3
  40.7 0.5 collective-permute-done
  41.2 4.3 %collective-permute-done.1 = bf16[256,15]{1,0:T(8,128)(2,1)S(1)} collective-permute-done((bf16[256,15]{1,0:T(8,128)(2,1)S(1)}, bf16[256,15]{1,0:T(8,128)(2,1)S(1)}, u32[]{:S(2)}, u32[]{:S(2)}) %collective-permute-start.1) | collective-permute-done | bytes 7712 | tf_op jit(solution)/shard_map/ppermute | solution.py:17
  45.5 0.2 maximum_convert_fusion
  45.7 6.5 %fusion.33 = bf16[256,512]{1,0:T(8,128)(2,1)} fusion(f32[256,542]{1,0:T(8,128)S(1)} %maximum_convert_fusion, f32[256]{0:T(256)S(1)} %bitcast.97, f32[256]{0:T(256)S(1)} %bitcast.96, f32[256]{0:T(256)S(1)} %bitcast.95, f32[256]{0:T(256)S(1)} %bitcast.94, f32[256]{0:T(256)S(1)} %bitcast.93, f32[256]{0:T(256)S(1)} %bitcast.92, f32[256]{0:T(256)S(1)} %bitcast.91, ...), kind=kLoop, calls=%fused_computation.34 | loop fusion | flops 8126464 | bytes 16546816 | tf_op jit(solution)/shard_map/convert_element_type | solution.py:65
  52.2 0.0 all-gather.4.cloned.1.call-update
  52.2 0.0 all-gather.8.cloned.1.call-start
  52.3 5.2 %all-gather.6.cloned.1.call-done = bf16[256,4096]{1,0:T(8,128)(2,1)} async-done(((bf16[256,1024]{1,0:T(8,128)(2,1)}), bf16[256,4096]{1,0:T(8,128)(2,1)}) %all-gather.6.cloned.1.call-update) | async-done | bytes 2097168 | tf_op jit(solution)/shard_map/all_gather | solution.py:80
  57.4 0.0 copy-start.6
  57.4 0.0 copy-start.7
  57.4 4.2 %fusion.4 = f32[256,512]{1,0:T(8,128)S(1)} fusion(bf16[256,4096]{1,0:T(8,128)(2,1)} %all-gather.6.cloned.1.call-done, bf16[1,4096,512]{2,1,0:T(8,128)(2,1)} %param.23), kind=kOutput, calls=%fused_computation.7 | convolution fusion | flops 1073741824 | bytes 6815744 | tf_op jit(solution)/shard_map/dot_general | solution.py:81
  61.7 0.0 copy-done.6
  61.7 0.5 copy-done.7
  62.1 0.0 copy-start.4
  62.1 0.0 copy-start.5
  62.1 2.0 %fusion.23 = bf16[256,512]{1,0:T(8,128)(2,1)} fusion(bf16[256,4096]{1,0:T(8,128)(2,1)S(1)} %copy-done.7, bf16[1,4096,512]{2,1,0:T(8,128)(2,1)S(1)} %copy-done.6, f32[256,512]{1,0:T(8,128)S(1)} %fusion.4), kind=kOutput, calls=%fused_computation.25 | convolution fusion | flops 1074528256 | bytes 7077888 | tf_op jit(solution)/shard_map/dot_general | solution.py:82
  64.1 0.0 all-gather.8.cloned.1.call-update
  64.1 0.0 copy-done.4
  64.2 0.0 copy-done.5
  64.2 0.1 copy.19
  64.3 12.0 %all-gather.4.cloned.1.call-done = bf16[1024,512]{1,0:T(8,128)(2,1)} async-done(((bf16[256,512]{1,0:T(8,128)(2,1)}), bf16[1024,512]{1,0:T(8,128)(2,1)}) %all-gather.4.cloned.1.call-update) | async-done | bytes 1048592 | tf_op jit(solution)/shard_map/all_gather | solution.py:85
  76.3 1.4 %convert_reduce_fusion = f32[512]{0:T(512)S(1)} fusion(bf16[1024,512]{1,0:T(8,128)(2,1)} %all-gather.4.cloned.1.call-done), kind=kLoop, calls=%fused_computation.10 | loop fusion | flops 1048064 | bytes 1050624 | tf_op jit(solution)/shard_map/reduce_sum | solution.py:26
  77.7 17.4 %all-gather.8.cloned.1.call-done = bf16[256,2048]{1,0:T(8,128)(2,1)} async-done(((bf16[256,512]{1,0:T(8,128)(2,1)}), bf16[256,2048]{1,0:T(8,128)(2,1)}) %all-gather.8.cloned.1.call-update) | async-done | bytes 1048592 | tf_op jit(solution)/shard_map/all_gather | solution.py:87
  95.2 4.6 %fusion.17 = bf16[256,1024]{1,0:T(8,128)(2,1)} fusion(bf16[256,2048]{1,0:T(8,128)(2,1)} %all-gather.8.cloned.1.call-done, bf16[1,2048,1024]{2,1,0:T(8,128)(2,1)} %param.25), kind=kOutput, calls=%fused_computation.23 | convolution fusion | flops 1074003968 | bytes 5767168 | tf_op jit(solution)/shard_map/dot_general | solution.py:86
  99.8 0.0 copy-start.8
  99.8 0.0 copy-start.9
  99.8 5.6 %all-to-all-start.1 = ((bf16[8,32,1024]{2,1,0:T(8,128)(2,1)}), bf16[8,32,1024]{2,1,0:T(8,128)(2,1)S(1)}, u32[]{:S(2)}, u32[]{:S(2)}) async-start(bf16[8,32,1024]{2,1,0:T(8,128)(2,1)} %bitcast.40), calls=%async_computation.1 | async-start | bytes 1048576 | tf_op jit(solution)/shard_map/all_to_all | solution.py:91
  105.4 1.6 %fusion.8 = f32[512]{0:T(512)S(1)} fusion(bf16[1024,512]{1,0:T(8,128)(2,1)} %all-gather.4.cloned.1.call-done, f32[512]{0:T(512)S(1)} %broadcast_multiply_fusion), kind=kLoop, calls=%fused_computation.13 | loop fusion | flops 2096640 | bytes 1052672 | tf_op jit(solution)/shard_map/reduce_sum | solution.py:27
  107.0 0.0 copy-done
  107.0 0.0 copy-done.8
  107.0 0.0 copy-done.9
  107.0 3.7 %convolution_convert_fusion = bf16[512,1024]{1,0:T(8,128)(2,1)} fusion(bf16[1024,1024]{1,0:T(8,128)(2,1)S(1)} %copy-done, bf16[1024,512]{1,0:T(8,128)(2,1)} %all-gather.4.cloned.1.call-done, f32[1024]{0:T(1024)S(1)} %copy-done.8, f32[1024]{0:T(1024)S(1)} %copy-done.9, f32[512]{0:T(512)S(1)} %add_rsqrt_fusion, f32[512]{0:T(512)S(1)} %broadcast_multiply_fusion), kind=kOutput, calls=%fused_computation.22 | convolution fusion | flops 1079508992 | bytes 4206592 | tf_op jit(solution)/shard_map/dot_general | solution.py:98
  110.7 9.5 %all-to-all-done.1 = bf16[8,32,1024]{2,1,0:T(8,128)(2,1)S(1)} async-done(((bf16[8,32,1024]{2,1,0:T(8,128)(2,1)}), bf16[8,32,1024]{2,1,0:T(8,128)(2,1)S(1)}, u32[]{:S(2)}, u32[]{:S(2)}) %all-to-all-start.1) | async-done | bytes 524320 | tf_op jit(solution)/shard_map/all_to_all | solution.py:91
  120.3 2.0 %gather_fusion.1 = bf16[256,1024]{1,0:T(8,128)(2,1)} fusion(bf16[256,1024]{1,0:T(8,128)(2,1)S(1)} %bitcast.64, s32[1024]{0:T(1024)S(1)} %pad_clamp_fusion), kind=kCustom, calls=%fused_computation.1 | custom fusion | bytes 1049600 | tf_op jit(solution)/shard_map/gather | solution.py:94
  122.2 1.7 %reshape.133 = f32[128,2,1024]{2,1,0:T(2,128)S(1)} reshape(bf16[256,1024]{1,0:T(8,128)(2,1)} %gather_fusion.1) | data formatting | bytes 1572864 | tf_op jit(solution)/shard_map/convert_element_type | solution.py:94
  123.9 2.1 %multiply_reduce_fusion = bf16[128,1024]{1,0:T(8,128)(2,1)} fusion(f32[128,2,1024]{2,1,0:T(2,128)S(1)} %reshape.133, f32[128,2]{1,0:T(8,128)S(1)} %copy.19), kind=kLoop, calls=%fused_computation.26 | loop fusion | flops 393216 | bytes 1311744 | tf_op jit(solution)/shard_map/reduce_sum | solution.py:96
  (14 shorter events, 0.1 us)
Async XLA Ops:
  7.2 99.8 %copy-start = (bf16[1024,1024]{1,0:T(8,128)(2,1)S(1)}, bf16[1024,1024]{1,0:T(8,128)(2,1)}, u32[]{:S(2)}) copy-start(bf16[1024,1024]{1,0:T(8,128)(2,1)} %param.18) | copy-start | bytes 6291460
  7.2 50.3 %all-gather.6.cloned.1.call-start = ((), (), s32[]{:S(2)}) async-start(), calls=%async_computation.3 | async-start | bytes 2621440 | tf_op jit(solution)/shard_map/all_gather | solution.py:80
  12.7 23.0 %copy-start.1 = (bf16[256,512]{1,0:T(8,128)(2,1)S(1)}, bf16[256,512]{1,0:T(8,128)(2,1)}, u32[]{:S(2)}) copy-start(bf16[256,512]{1,0:T(8,128)(2,1)} %param.14) | copy-start | bytes 786436
  12.7 23.0 %copy-start.2 = (bf16[256,512]{1,0:T(8,128)(2,1)S(1)}, bf16[256,512]{1,0:T(8,128)(2,1)}, u32[]{:S(2)}) copy-start(bf16[256,512]{1,0:T(8,128)(2,1)} %param.13) | copy-start | bytes 786436
  13.9 26.7 %copy-start.3 = (bf16[31,256]{1,0:T(8,128)(2,1)S(1)}, bf16[31,256]{1,0:T(8,128)(2,1)}, u32[]{:S(2)}) copy-start(bf16[31,256]{1,0:T(8,128)(2,1)} %param.15) | copy-start | bytes 47620
  35.7 40.6 %all-gather.4.cloned.1.call-start = ((), (), s32[]{:S(2)}) async-start(), calls=%async_computation.2 | async-start | bytes 1310720 | tf_op jit(solution)/shard_map/all_gather | solution.py:85
  36.0 5.2 %collective-permute-start = (bf16[256,15]{1,0:T(8,128)(2,1)S(1)}, bf16[256,15]{1,0:T(8,128)(2,1)S(1)}, u32[]{:S(2)}, u32[]{:S(2)}) collective-permute-start(bf16[256,15]{1,0:T(8,128)(2,1)S(1)} %get-tuple-element.4), channel_id=1, source_target_pairs={{0,4},{4,8},{8,12},{12,16},{16,20},{20,24},{24,28},{1,5},{5,9},{9,... | collective-permute-start | bytes 23048 | tf_op jit(solution)/shard_map/ppermute | solution.py:15
  39.3 6.2 %collective-permute-start.1 = (bf16[256,15]{1,0:T(8,128)(2,1)S(1)}, bf16[256,15]{1,0:T(8,128)(2,1)S(1)}, u32[]{:S(2)}, u32[]{:S(2)}) collective-permute-start(bf16[256,15]{1,0:T(8,128)(2,1)S(1)} %get-tuple-element.5), channel_id=1, source_target_pairs={{4,0},{8,4},{12,8},{16,12},{20,16},{24,20},{28,24},{5,1},{9,5},{13... | collective-permute-start | bytes 23048 | tf_op jit(solution)/shard_map/ppermute | solution.py:17
  52.2 43.0 %all-gather.8.cloned.1.call-start = ((), (), s32[]{:S(2)}) async-start(), calls=%async_computation.4 | async-start | bytes 1310720 | tf_op jit(solution)/shard_map/all_gather | solution.py:87
  57.4 4.2 %copy-start.6 = (bf16[1,4096,512]{2,1,0:T(8,128)(2,1)S(1)}, bf16[1,4096,512]{2,1,0:T(8,128)(2,1)}, u32[]{:S(2)}) copy-start(bf16[1,4096,512]{2,1,0:T(8,128)(2,1)} %param.24) | copy-start | bytes 12582916
  57.4 4.7 %copy-start.7 = (bf16[256,4096]{1,0:T(8,128)(2,1)S(1)}, bf16[256,4096]{1,0:T(8,128)(2,1)}, u32[]{:S(2)}) copy-start(bf16[256,4096]{1,0:T(8,128)(2,1)} %all-gather.6.cloned.1.call-done) | copy-start | bytes 6291460
  62.1 2.0 %copy-start.4 = (f32[128,2]{0,1:T(2,128)S(1)}, f32[128,2]{0,1:T(2,128)}, u32[]{:S(2)}) copy-start(f32[128,2]{0,1:T(2,128)} %param.21) | copy-start | bytes 3076
  62.1 2.0 %copy-start.5 = (f32[128]{0:T(128)S(1)}, f32[128]{0:T(128)}, u32[]{:S(2)}) copy-start(f32[128]{0:T(128)} %param.22) | copy-start | bytes 1540
  99.8 7.2 %copy-start.8 = (f32[1024]{0:T(1024)S(1)}, f32[1024]{0:T(1024)}, u32[]{:S(2)}) copy-start(f32[1024]{0:T(1024)} %param.17) | copy-start | bytes 12292
  99.8 7.2 %copy-start.9 = (f32[1024]{0:T(1024)S(1)}, f32[1024]{0:T(1024)}, u32[]{:S(2)}) copy-start(f32[1024]{0:T(1024)} %param.16) | copy-start | bytes 12292
  99.8 20.5 %all-to-all-start.1 = ((bf16[8,32,1024]{2,1,0:T(8,128)(2,1)}), bf16[8,32,1024]{2,1,0:T(8,128)(2,1)S(1)}, u32[]{:S(2)}, u32[]{:S(2)}) async-start(bf16[8,32,1024]{2,1,0:T(8,128)(2,1)} %bitcast.40), calls=%async_computation.1 | async-start | bytes 1048576 | tf_op jit(solution)/shard_map/all_to_all | solution.py:91
Sparse Core Ops, SparseCore 0:
  35.8 21.5 all-gather.5
  59.6 16.6 all-gather.3
  78.4 16.6 all-gather.7
where the time goes:
time: 133 us
  waiting for transfers between devices  49 us (37%)
  blocking collectives  21.7 us (16%)
  matrix products  14.5 us (11%)
  between operations  14 us (11%)
  other arithmetic  13.4 us (10%)
  starting transfers between devices  10.4 us (8%)
  local copies, waits for them, and re-layouts  9.64 us (7%)
    all_to_all x1, blocking collectives, local(): lax.all_to_all(columns[source_row], 'ep', split_axis=0, concat_axis=0, ti...  21.7 us
    all_gather x1, waiting for transfers between devices, local(): lax.all_gather(hidden, 'tp', axis=1, tiled=True)  17.4 us
    all_gather x1, waiting for transfers between devices, local(): whole_conv = lax.all_gather(conv_out, 'tp', axis=0, tiled=True)  12 us
    all_to_all x1, waiting for transfers between devices, local(): lax.all_to_all(produced.astype(jnp.bfloat16), 'ep', split_axis=0, concat_...  9.54 us
    convert_element_type x1, other arithmetic, local(): conv_out = summed.astype(jnp.bfloat16)  6.5 us
    all_to_all x1, starting transfers between devices, local(): lax.all_to_all(produced.astype(jnp.bfloat16), 'ep', split_axis=0, concat_...  5.64 us
    all_gather x1, waiting for transfers between devices, local(): arrived = lax.all_gather(sliced, 'tp', axis=1, tiled=True)  5.18 us
    dot_general x1, matrix products, local(): jnp.dot(lax.all_gather(hidden, 'tp', axis=1, tiled=True), down_local, pre...  4.57 us
  transfers between devices with their start and end apart: 6, of which 6 were waited for; matrix products, arithmetic and copies ran while one was open for 15% of the time, Pallas kernels for 0%

commit v1 on v0

v1 whole, which is shorter than its diff:
```python
import functools

import jax
import jax.numpy as jnp
from jax import lax
from jax.experimental import pallas as pl
from jax.experimental.pallas import tpu as pltpu
from jax.sharding import PartitionSpec as P

MESH = pl.DeviceIdType.MESH
CORES = 2
F32, BF16 = jnp.float32, jnp.bfloat16


def tiles(size, most):
    tile = min(size, most)
    return tile, size // tile


def kernel(
    experts,
    parts,
    value_hbm,
    gate_hbm,
    input_hbm,
    wgate_hbm,
    wup_hbm,
    wdown_hbm,
    wout_hbm,
    taps_ref,
    gain_ref,
    shift_ref,
    ids_ref,
    logits_ref,
    prob_ref,
    mixer_hbm,
    expert_hbm,
    value,
    gate,
    tokens,
    wgate,
    wup,
    wdown,
    wout,
    send_rows,
    arrived,
    gate_sum,
    up_sum,
    hidden,
    down_sum,
    result,
    returned,
    padded,
    edges,
    halo,
    conv,
    swished,
    mixer,
    combined,
    load_sem,
    out_sem,
    self_sem,
    disp_send,
    disp_recv,
    fwd_send,
    fwd_recv,
    hal_send,
    hal_recv,
    conv_send,
    conv_recv,
    hid_send,
    hid_recv,
    ret_send,
    ret_recv,
):
    me = lax.axis_index("ep")
    tp = lax.axis_index("tp")
    chips = parts // CORES
    chip, core = lax.div(tp, CORES), lax.rem(tp, CORES)
    other = 1 - core
    sibling = chip * CORES + other
    slots = send_rows.shape[1]
    half = send_rows.shape[2]
    rows = experts * slots
    length, channels = conv.shape[1], conv.shape[2]
    edge = halo.shape[1]
    reach = (taps_ref.shape[0] - 1) // 2

    def remote(src, dst, ssem, rsem, ep=None, part=None):
        target = (me if ep is None else ep, tp if part is None else part)
        return pltpu.make_async_remote_copy(
            src_ref=src, dst_ref=dst, send_sem=ssem, recv_sem=rsem, device_id=target, device_id_type=MESH
        )

    def ahead(k):
        return lax.rem(me + k, experts)

    def behind(k):
        return lax.rem(me + experts - k, experts)

    def chip_ahead(k):
        return lax.rem(chip + k, chips) * CORES + core

    def chip_behind(k):
        return lax.rem(chip + chips - k, chips) * CORES + core

    barrier = pltpu.get_barrier_semaphore()

    @pl.loop(1, experts)
    def _(k):
        pl.semaphore_signal(barrier, inc=1, device_id=(ahead(k), tp), device_id_type=MESH)

    @pl.loop(1, chips)
    def _(k):
        pl.semaphore_signal(barrier, inc=1, device_id=(me, chip_ahead(k)), device_id_type=MESH)

    pl.semaphore_signal(barrier, inc=1, device_id=(me, sibling), device_id_type=MESH)

    columns = pl.ds(pl.multiple_of(core * half, half), half)
    loads = [
        pltpu.make_async_copy(src, dst, load_sem.at[i])
        for i, (src, dst) in enumerate(
            [
                (input_hbm.at[:, columns], tokens),
                (value_hbm, value),
                (gate_hbm, gate),
                (wgate_hbm.at[0], wgate),
                (wup_hbm.at[0], wup),
                (wout_hbm, wout),
                (wdown_hbm.at[0], wdown),
            ]
        )
    ]
    for load in loads:
        load.start()

    count = ids_ref.shape[1]
    first, second = ids_ref[0:1, :], ids_ref[1:2, :]
    expert_of = lax.broadcasted_iota(jnp.int32, (experts, count), 0)
    is_first, is_second = expert_of == first, expert_of == second
    chosen = jnp.where(is_first | is_second, 1.0, 0.0).astype(F32)
    earlier = lax.broadcasted_iota(jnp.int32, (count, count), 0) < lax.broadcasted_iota(
        jnp.int32, (count, count), 1
    )
    rank = jnp.dot(
        chosen.astype(BF16), jnp.where(earlier, 1.0, 0.0).astype(BF16), preferred_element_type=F32
    )
    rank = jnp.where(chosen > 0, rank, -1.0)
    ordinal = lax.broadcasted_iota(jnp.int32, (experts, slots, count), 1).astype(F32)
    place3 = jnp.broadcast_to(rank[:, None, :], (experts, slots, count)) == ordinal
    place = jnp.where(place3, 1.0, 0.0).astype(F32).reshape(rows, count)

    loads[0].wait()
    tile, steps = tiles(half, 512)
    for i in range(steps):
        span = slice(i * tile, (i + 1) * tile)
        picked = jnp.dot(place.astype(BF16), tokens[:, span], preferred_element_type=F32)
        send_rows[:, :, span] = picked.reshape(experts, slots, tile).astype(BF16)

    pl.semaphore_wait(barrier, experts - 1 + chips)

    def dispatch(k):
        return remote(
            send_rows.at[ahead(k)], arrived.at[core, me], disp_send.at[k], disp_recv.at[k], ep=ahead(k)
        )

    def forward(k, src):
        return remote(
            src, arrived.at[core, behind(k)], fwd_send.at[k], fwd_recv.at[k], part=sibling
        )

    @pl.loop(1, experts)
    def _(k):
        dispatch(k).start()

    keep = pltpu.make_async_copy(send_rows.at[me], arrived.at[core, me], self_sem.at[0])
    keep.start()
    forward(0, send_rows.at[me]).start()

    loads[1].wait()
    loads[2].wait()
    gated = (value[...].astype(F32) * jax.nn.sigmoid(gate[...].astype(F32))).astype(BF16)
    padded[edge : edge + length, :] = jnp.transpose(gated.astype(F32), (1, 0))
    edges[0] = padded[edge : 2 * edge, :].astype(BF16)
    edges[1] = padded[length : length + edge, :].astype(BF16)
    to_left = remote(edges.at[0], halo.at[1], hal_send.at[0], hal_recv.at[0], ep=behind(1))
    to_right = remote(edges.at[1], halo.at[0], hal_send.at[1], hal_recv.at[1], ep=ahead(1))
    to_left.start()
    to_right.start()
    taps = taps_ref[...].astype(F32)
    chunk, chunks = tiles(length, 64)

    def convolve(i):
        total = jnp.zeros((chunk, channels), F32)
        for j in range(taps.shape[0]):
            start = i * chunk + j + edge - reach
            total = total + taps[j : j + 1, :] * padded[start : start + chunk, :]
        conv[tp, i * chunk : (i + 1) * chunk, :] = total.astype(BF16)

    for i in range(1, chunks - 1):
        convolve(i)
    to_left.wait()
    to_right.wait()
    padded[0:edge, :] = jnp.where(me == 0, 0.0, halo[0].astype(F32))
    padded[edge + length : 2 * edge + length, :] = jnp.where(
        me == experts - 1, 0.0, halo[1].astype(F32)
    )
    convolve(0)
    convolve(chunks - 1)

    def gather(buffer, ssem, rsem):
        def across(k):
            return remote(buffer.at[tp], buffer.at[tp], ssem.at[k], rsem.at[k], part=chip_ahead(k))

        def beside(k):
            block = chip_behind(k)
            return remote(
                buffer.at[block], buffer.at[block], ssem.at[chips + k], rsem.at[chips + k], part=sibling
            )

        return across, beside

    conv_across, conv_beside = gather(conv, conv_send, conv_recv)

    @pl.loop(1, chips)
    def _(k):
        conv_across(k).start()

    conv_beside(0).start()

    @pl.loop(1, experts)
    def _(k):
        dispatch(k).wait_recv()
        forward(k, arrived.at[core, behind(k)]).start()

    keep.wait()
    loads[3].wait()
    loads[4].wait()
    units = gate_sum.shape[1]
    tile, steps = tiles(units, 256)

    def side(which):
        block = arrived[which]
        if slots % 16:
            return block.astype(F32).reshape(rows, half).astype(BF16)
        return block.reshape(rows, half)

    def depth(which):
        return pl.ds(pl.multiple_of(which * half, half), half)

    for i in range(steps):
        span = slice(i * tile, (i + 1) * tile)
        gate_sum[:, span] = jnp.dot(side(core), wgate[depth(core), span], preferred_element_type=F32)
        up_sum[:, span] = jnp.dot(side(core), wup[depth(core), span], preferred_element_type=F32)

    @pl.loop(0, experts)
    def _(k):
        forward(k, send_rows.at[me]).wait_recv()

    for i in range(steps):
        span = slice(i * tile, (i + 1) * tile)
        gate_val = gate_sum[:, span] + jnp.dot(
            side(other), wgate[depth(other), span], preferred_element_type=F32
        )
        up_val = up_sum[:, span] + jnp.dot(
            side(other), wup[depth(other), span], preferred_element_type=F32
        )
        hidden[tp, :, span] = (jax.nn.silu(gate_val) * up_val).astype(BF16)

    hid_across, hid_beside = gather(hidden, hid_send, hid_recv)

    @pl.loop(1, chips)
    def _(k):
        hid_across(k).start()

    hid_beside(0).start()

    @pl.loop(1, chips)
    def _(k):
        conv_across(k).wait_recv()
        conv_beside(k).start()

    @pl.loop(0, chips)
    def _(k):
        conv_beside(k).wait_recv()

    width = parts * channels
    chunk, chunks = tiles(length, 64)

    @pl.loop(0, chunks)
    def _(i):
        span = pl.ds(pl.multiple_of(i * chunk, chunk), chunk)
        blocks = [conv[b, span, :].astype(F32) for b in range(parts)]
        center = sum(jnp.sum(block, axis=1, keepdims=True) for block in blocks) / width
        blocks = [block - center for block in blocks]
        spread = sum(jnp.sum(block * block, axis=1, keepdims=True) for block in blocks) / width
        scale = lax.rsqrt(spread + 1e-05)
        for b in range(parts):
            lanes = slice(b * channels, (b + 1) * channels)
            normed = blocks[b] * scale * gain_ref[:, lanes] + shift_ref[:, lanes]
            swished[b, span, :] = jax.nn.silu(normed).astype(BF16)

    loads[6].wait()
    wide = down_sum.shape[1]
    tile, steps = tiles(wide, 256)

    def down(block, begin):
        deep = pl.ds(pl.multiple_of(block * units, units), units)

        @pl.loop(0, steps)
        def _(i):
            span = pl.ds(pl.multiple_of(i * tile, tile), tile)
            product = jnp.dot(hidden[block], wdown[deep, span], preferred_element_type=F32)
            down_sum[:, span] = product if begin else down_sum[:, span] + product

    down(tp, True)
    hid_beside(0).wait_recv()
    down(sibling, False)

    @pl.loop(1, chips)
    def _(k):
        hid_across(k).wait_recv()
        hid_beside(k).start()
        down(chip_behind(k), False)
        hid_beside(k).wait_recv()
        down(chip_behind(k) + other - core, False)

    result[...] = down_sum[...].reshape(experts, slots, wide).astype(BF16)

    def give_back(k):
        return remote(result.at[ahead(k)], returned.at[me], ret_send.at[k], ret_recv.at[k], ep=ahead(k))

    @pl.loop(1, experts)
    def _(k):
        give_back(k).start()

    own = pltpu.make_async_copy(result.at[me], returned.at[me], self_sem.at[1])
    own.start()

    loads[5].wait()
    tile, steps = tiles(mixer.shape[1], 256)

    @pl.loop(0, steps)
    def _(i):
        span = pl.ds(pl.multiple_of(i * tile, tile), tile)
        total = jnp.zeros((length, tile), F32)
        for b in range(parts):
            total = total + jnp.dot(
                swished[b], wout[b * channels : (b + 1) * channels, span], preferred_element_type=F32
            )
        mixer[:, span] = total.astype(BF16)

    put_mixer = pltpu.make_async_copy(mixer, mixer_hbm, out_sem.at[0])
    put_mixer.start()

    share = jax.nn.sigmoid(logits_ref[0:1, :] - logits_ref[1:2, :])
    weight = jnp.where(is_first, share * prob_ref[...], 0.0) + jnp.where(
        is_second, (1.0 - share) * prob_ref[...], 0.0
    )
    weights = jnp.where(
        place3, jnp.broadcast_to(weight[:, None, :], (experts, slots, count)), 0.0
    ).reshape(rows, count)
    weights = jnp.transpose(weights, (1, 0))
    high = weights.astype(BF16)
    rest = weights - high.astype(F32)
    middle = rest.astype(BF16)
    low = (rest - middle.astype(F32)).astype(BF16)

    own.wait()

    @pl.loop(1, experts)
    def _(k):
        give_back(k).wait_recv()

    tile, steps = tiles(wide, 512)
    for i in range(steps):
        span = slice(i * tile, (i + 1) * tile)
        block = returned[:, :, span]
        if slots % 16:
            block = block.astype(F32).reshape(rows, tile).astype(BF16)
        else:
            block = block.reshape(rows, tile)
        total = jnp.dot(low, block, preferred_element_type=F32)
        total = total + jnp.dot(middle, block, preferred_element_type=F32)
        total = total + jnp.dot(high, block, preferred_element_type=F32)
        combined[:, span] = total.astype(BF16)

    put_expert = pltpu.make_async_copy(combined, expert_hbm, out_sem.at[1])
    put_expert.start()

    @pl.loop(1, experts)
    def _(k):
        dispatch(k).wait_send()
        give_back(k).wait_send()

    @pl.loop(0, experts)
    def _(k):
        forward(k, send_rows.at[me]).wait_send()

    @pl.loop(1, chips)
    def _(k):
        conv_across(k).wait_send()
        hid_across(k).wait_send()

    @pl.loop(0, chips)
    def _(k):
        conv_beside(k).wait_send()
        hid_beside(k).wait_send()

    put_mixer.wait()
    put_expert.wait()


def local(
    experts,
    parts,
    conv_value,
    conv_gate,
    conv_kernel,
    norm_gain,
    norm_shift,
    out_weight,
    expert_input,
    expert_ids,
    pair_logits,
    group_prob,
    expert_gate,
    expert_up,
    expert_down,
):
    channels, length = conv_value.shape
    count, model = expert_input.shape
    slots = 2 * count // experts
    rows = experts * slots
    half = model // CORES
    units, wide = expert_gate.shape[2], expert_down.shape[2]
    out_width = out_weight.shape[1]
    chips = parts // CORES
    edge = -(-((conv_kernel.shape[0] - 1) // 2) // 16) * 16
    anywhere = pl.BlockSpec(memory_space=pl.ANY)
    near = pl.BlockSpec(memory_space=pltpu.VMEM)
    dma = pltpu.SemaphoreType.DMA
    return pl.pallas_call(
        functools.partial(kernel, experts, parts),
        out_shape=(
            jax.ShapeDtypeStruct((length, out_width), BF16),
            jax.ShapeDtypeStruct((count, wide), BF16),
        ),
        in_specs=[anywhere] * 7 + [near] * 6,
        out_specs=(anywhere, anywhere),
        scratch_shapes=[
            pltpu.VMEM((channels, length), BF16),
            pltpu.VMEM((channels, length), BF16),
            pltpu.VMEM((count, half), BF16),
            pltpu.VMEM((model, units), BF16),
            pltpu.VMEM((model, units), BF16),
            pltpu.VMEM(expert_down.shape[1:], BF16),
            pltpu.VMEM(out_weight.shape, BF16),
            pltpu.VMEM((experts, slots, half), BF16),
            pltpu.VMEM((CORES, experts, slots, half), BF16),
            pltpu.VMEM((rows, units), F32),
            pltpu.VMEM((rows, units), F32),
            pltpu.VMEM((parts, rows, units), BF16),
            pltpu.VMEM((rows, wide), F32),
            pltpu.VMEM((experts, slots, wide), BF16),
            pltpu.VMEM((experts, slots, wide), BF16),
            pltpu.VMEM((length + 2 * edge, channels), F32),
            pltpu.VMEM((2, edge, channels), BF16),
            pltpu.VMEM((2, edge, channels), BF16),
            pltpu.VMEM((parts, length, channels), BF16),
            pltpu.VMEM((parts, length, channels), BF16),
            pltpu.VMEM((length, out_width), BF16),
            pltpu.VMEM((count, wide), BF16),
            dma((7,)),
            dma((2,)),
            dma((2,)),
            dma((experts,)),
            dma((experts,)),
            dma((experts,)),
            dma((experts,)),
            dma((2,)),
            dma((2,)),
            dma((2 * chips,)),
            dma((2 * chips,)),
            dma((2 * chips,)),
            dma((2 * chips,)),
            dma((experts,)),
            dma((experts,)),
        ],
        compiler_params=pltpu.CompilerParams(
            collective_id=0, has_side_effects=True, vmem_limit_bytes=60 * 1024 * 1024
        ),
        name="block",
    )(
        conv_value,
        conv_gate,
        expert_input,
        expert_gate,
        expert_up,
        expert_down,
        out_weight,
        conv_kernel,
        norm_gain[None, :],
        norm_shift[None, :],
        expert_ids.T,
        pair_logits.T,
        group_prob[None, :],
    )


def solution(mesh):
    placed = (
        P("tp", "ep"),
        P("tp", "ep"),
        P(None, "tp"),
        P(),
        P(),
        P(None, "tp"),
        P("ep", None),
        P("ep", None),
        P("ep", None),
        P("ep"),
        P("ep", None, "tp"),
        P("ep", None, "tp"),
        P("ep", None, "tp"),
    )
    return jax.shard_map(
        functools.partial(local, mesh.shape["ep"], mesh.shape["tp"]),
        mesh=mesh,
        in_specs=placed,
        out_specs=(P("ep", "tp"), P("ep", "tp")),
        check_vma=False,
    )
```

time: 133 us -> 61.3 us (0.46)
  the two profiles are of different devices: /device:TPU:0 before, /device:TPU:11 now
where the time goes in v1:
time: 61.3 us; the launch traced here: 61 us
  Pallas kernels  56.5 us (92%)
  local copies, waits for them, and re-layouts  3.93 us (6%)
  between operations  0.64 us (1%)
    pallas_call x1, Pallas kernels, local(): pl.pallas_call(functools.partial(kernel, experts, parts), out_shape=(jax....  56.5 us
    unnamed x2, local copies, waits for them, and re-layouts  3.93 us

profile of v1, /device:TPU:11, one launch (start us, length us, event | category | flops | bytes accessed | tf_op | source)
XLA Modules:
  0.0 61.0 jit_solution(4138205458891743859)
XLA Ops:
  0.6 56.5 %block.1 = (bf16[512,1024]{1,0:T(8,128)(2,1)}, bf16[128,1024]{1,0:T(8,128)(2,1)}) custom-call(bf16[256,512]{1,0:T(8,128)(2,1)} %value_hbm.1, bf16[256,512]{1,0:T(8,128)(2,1)} %gate_hbm.1, bf16[128,4096]{1,0:T(8,128)(2,1)} %input_hbm.1, bf16[1,4096,512]{2,1,0:T(8,128)(2,1)} %wgate_hbm.1, bf16[1,4096,512]{2,1,0:T(8,128)(2,1)} %wup_hbm.1, ...), custom_call_target="tpu_custom_call" | custom-call | tf_op jit(solution)/shard_map/block/pallas_call | solution.py:443
  57.1 2.3 %copy.17 = bf16[512,1024]{1,0:T(8,128)(2,1)} copy(bf16[512,1024]{1,0:T(8,128)(2,1)} %get-tuple-element.4) | data formatting | bytes 2097152
  59.4 1.7 %copy.18 = bf16[128,1024]{1,0:T(8,128)(2,1)} copy(bf16[128,1024]{1,0:T(8,128)(2,1)} %get-tuple-element.5) | data formatting | bytes 524288

commit v2 on v1

--- a/solution.py
+++ b/solution.py
@@ -44,8 +44,6 @@
     wout,
     send_rows,
     arrived,
-    gate_sum,
-    up_sum,
     hidden,
     down_sum,
     result,
@@ -62,8 +60,10 @@
     self_sem,
     disp_send,
     disp_recv,
-    fwd_send,
-    fwd_recv,
+    side_send,
+    side_recv,
+    far_send,
+    far_recv,
     hal_send,
     hal_recv,
     conv_send,
@@ -80,7 +80,10 @@
     other = 1 - core
     sibling = chip * CORES + other
     slots = send_rows.shape[1]
-    half = send_rows.shape[2]
+    part_width = send_rows.shape[2]
+    near = experts // 2
+    base = lax.div(me, near) * near
+    place_in = lax.rem(me, near)
     rows = experts * slots
     length, channels = conv.shape[1], conv.shape[2]
     edge = halo.shape[1]
@@ -116,7 +119,7 @@
 
     pl.semaphore_signal(barrier, inc=1, device_id=(me, sibling), device_id_type=MESH)
 
-    columns = pl.ds(pl.multiple_of(core * half, half), half)
+    columns = pl.ds(pl.multiple_of(tp * part_width, part_width), part_width)
     loads = [
         pltpu.make_async_copy(src, dst, load_sem.at[i])
         for i, (src, dst) in enumerate(
@@ -151,7 +154,7 @@
     place = jnp.where(place3, 1.0, 0.0).astype(F32).reshape(rows, count)
 
     loads[0].wait()
-    tile, steps = tiles(half, 512)
+    tile, steps = tiles(part_width, 512)
     for i in range(steps):
         span = slice(i * tile, (i + 1) * tile)
         picked = jnp.dot(place.astype(BF16), tokens[:, span], preferred_element_type=F32)
@@ -159,23 +162,47 @@
 
     pl.semaphore_wait(barrier, experts - 1 + chips)
 
-    def dispatch(k):
+    def partner(j, sign, crosses):
+        start = near - base if crosses else base
+        return start + lax.rem(place_in + near + sign * (j - near if crosses else j), near)
+
+    def dispatch(j, crosses):
+        to = partner(j, 1, crosses)
+        return remote(send_rows.at[to], arrived.at[tp, me], disp_send.at[j], disp_recv.at[j], ep=to)
+
+    def row_block(j, k, crosses):
+        return arrived.at[chip_behind(k), partner(j, -1, crosses)]
+
+    def to_side(j, k, crosses, src=None):
+        block = row_block(j, k, crosses)
+        at = k * experts + j
         return remote(
-            send_rows.at[ahead(k)], arrived.at[core, me], disp_send.at[k], disp_recv.at[k], ep=ahead(k)
+            block if src is None else src, block, side_send.at[at], side_recv.at[at], part=sibling
         )
 
-    def forward(k, src):
+    def to_far(j, k, crosses, src=None):
+        block = row_block(j, 0, crosses)
+        at = k * experts + j
         return remote(
-            src, arrived.at[core, behind(k)], fwd_send.at[k], fwd_recv.at[k], part=sibling
+            block if src is None else src, block, far_send.at[at], far_recv.at[at], part=chip_ahead(k)
         )
 
-    @pl.loop(1, experts)
-    def _(k):
-        dispatch(k).start()
-
-    keep = pltpu.make_async_copy(send_rows.at[me], arrived.at[core, me], self_sem.at[0])
+    def spread(j, crosses, src=None):
+        @pl.loop(1, chips)
+        def _(k):
+            to_far(j, k, crosses, src).start()
+
+        to_side(j, 0, crosses, src).start()
+
+    for crosses in (False, True):
+
+        @pl.loop(near if crosses else 1, experts if crosses else near)
+        def _(j):
+            dispatch(j, crosses).start()
+
+    keep = pltpu.make_async_copy(send_rows.at[me], arrived.at[tp, me], self_sem.at[0])
     keep.start()
-    forward(0, send_rows.at[me]).start()
+    spread(0, False, send_rows.at[me])
 
     loads[1].wait()
     loads[2].wait()
@@ -197,7 +224,8 @@
             total = total + taps[j : j + 1, :] * padded[start : start + chunk, :]
         conv[tp, i * chunk : (i + 1) * chunk, :] = total.astype(BF16)
 
-    for i in range(1, chunks - 1):
+    early = chunks // 2
+    for i in range(1, early):
         convolve(i)
     to_left.wait()
     to_right.wait()
@@ -205,75 +233,176 @@
     padded[edge + length : 2 * edge + length, :] = jnp.where(
         me == experts - 1, 0.0, halo[1].astype(F32)
     )
-    convolve(0)
-    convolve(chunks - 1)
-
-    def gather(buffer, ssem, rsem):
+
+    def gather(block_of, ssem, rsem):
         def across(k):
-            return remote(buffer.at[tp], buffer.at[tp], ssem.at[k], rsem.at[k], part=chip_ahead(k))
+            block = block_of(tp)
+            return remote(block, block, ssem(k), rsem(k), part=chip_ahead(k))
 
         def beside(k):
-            block = chip_behind(k)
-            return remote(
-                buffer.at[block], buffer.at[block], ssem.at[chips + k], rsem.at[chips + k], part=sibling
-            )
-
-        return across, beside
-
-    conv_across, conv_beside = gather(conv, conv_send, conv_recv)
-
-    @pl.loop(1, chips)
-    def _(k):
-        conv_across(k).start()
-
-    conv_beside(0).start()
-
-    @pl.loop(1, experts)
-    def _(k):
-        dispatch(k).wait_recv()
-        forward(k, arrived.at[core, behind(k)]).start()
-
+            block = block_of(chip_behind(k))
+            return remote(block, block, ssem(chips + k), rsem(chips + k), part=sibling)
+
+        def begin():
+            @pl.loop(1, chips)
+            def _(k):
+                across(k).start()
+
+            beside(0).start()
+
+        return across, beside, begin
+
+    conv_across, conv_beside, conv_begin = gather(
+        lambda b: conv.at[b], lambda k: conv_send.at[k], lambda k: conv_recv.at[k]
+    )
+
+    units = hidden.shape[3]
+    tile, steps = tiles(units, 256)
+    group_rows = near * slots
+
+    def join(block):
+        if slots % 16:
+            return block.astype(F32).reshape(group_rows, block.shape[-1]).astype(BF16)
+        return block.reshape(group_rows, block.shape[-1])
+
+    def arrive(j, crosses):
+        dispatch(j, crosses).wait_recv()
+        spread(j, crosses)
+
+    def relay(crosses):
+        @pl.loop(near if crosses else 0, experts if crosses else near)
+        def _(j):
+            @pl.loop(1, chips)
+            def _(k):
+                to_far(j, k, crosses).wait_recv()
+                to_side(j, k, crosses).start()
+
+    def settle(crosses):
+        @pl.loop(near if crosses else 0, experts if crosses else near)
+        def _(j):
+            @pl.loop(0, chips)
+            def _(k):
+                to_side(j, k, crosses).wait_recv()
+
+    def group(crosses):
+        mine = lax.div(me, near)
+        return (1 - mine) if crosses else mine
+
+    def members(crosses):
+        return pl.ds(group(crosses) * near, near)
+
+    def hidden_of(crosses):
+        g = group(crosses)
+        n = 1 if crosses else 0
+        return gather(
+            lambda b: hidden.at[b, g], lambda k: hid_send.at[n, k], lambda k: hid_recv.at[n, k]
+        )
+
+    def up_and_gate(crosses):
+        blocks = [join(arrived[p, members(crosses)]) for p in range(parts)]
+        for i in range(steps):
+            span = slice(i * tile, (i + 1) * tile)
+
+            def product(weights):
+                total = None
+                for p in range(parts):
+                    term = jnp.dot(
+                        blocks[p],
+                        weights[p * part_width : (p + 1) * part_width, span],
+                        preferred_element_type=F32,
+                    )
+                    total = term if total is None else total + term
+                return total
+
+            hidden[tp, group(crosses), :, span] = (
+                jax.nn.silu(product(wgate)) * product(wup)
+            ).astype(BF16)
+
+    @pl.loop(1, near)
+    def _(j):
+        arrive(j, False)
+
+    relay(False)
+    arrive(near, True)
     keep.wait()
     loads[3].wait()
     loads[4].wait()
-    units = gate_sum.shape[1]
-    tile, steps = tiles(units, 256)
-
-    def side(which):
-        block = arrived[which]
-        if slots % 16:
-            return block.astype(F32).reshape(rows, half).astype(BF16)
-        return block.reshape(rows, half)
-
-    def depth(which):
-        return pl.ds(pl.multiple_of(which * half, half), half)
-
-    for i in range(steps):
-        span = slice(i * tile, (i + 1) * tile)
-        gate_sum[:, span] = jnp.dot(side(core), wgate[depth(core), span], preferred_element_type=F32)
-        up_sum[:, span] = jnp.dot(side(core), wup[depth(core), span], preferred_element_type=F32)
-
-    @pl.loop(0, experts)
-    def _(k):
-        forward(k, send_rows.at[me]).wait_recv()
-
-    for i in range(steps):
-        span = slice(i * tile, (i + 1) * tile)
-        gate_val = gate_sum[:, span] + jnp.dot(
-            side(other), wgate[depth(other), span], preferred_element_type=F32
-        )
-        up_val = up_sum[:, span] + jnp.dot(
-            side(other), wup[depth(other), span], preferred_element_type=F32
-        )
-        hidden[tp, :, span] = (jax.nn.silu(gate_val) * up_val).astype(BF16)
-
-    hid_across, hid_beside = gather(hidden, hid_send, hid_recv)
-
-    @pl.loop(1, chips)
-    def _(k):
-        hid_across(k).start()
-
-    hid_beside(0).start()
+    settle(False)
+    up_and_gate(False)
+    near_across, near_beside, near_begin = hidden_of(False)
+    near_begin()
+
+    left = [0] + list(range(max(early, 1), chunks))
+    late = experts - near - 1
+    if late <= len(left):
+        for n in range(late):
+            arrive(near + 1 + n, True)
+            for i in left[n * len(left) // late : (n + 1) * len(left) // late]:
+                convolve(i)
+    else:
+
+        @pl.loop(near + 1, experts)
+        def _(j):
+            arrive(j, True)
+
+        for i in left:
+            convolve(i)
+
+    relay(True)
+    settle(True)
+    up_and_gate(True)
+    cross_across, cross_beside, cross_begin = hidden_of(True)
+    cross_begin()
+    conv_begin()
+
+    loads[6].wait()
+    wide = down_sum.shape[1]
+    tile, steps = tiles(wide, 256)
+
+    def give_back(j, crosses):
+        to = partner(j, 1, crosses)
+        return remote(result.at[to], returned.at[me], ret_send.at[j], ret_recv.at[j], ep=to)
+
+    def down(block, crosses, begin):
+        deep = pl.ds(pl.multiple_of(block * units, units), units)
+
+        @pl.loop(0, steps)
+        def _(i):
+            span = pl.ds(pl.multiple_of(i * tile, tile), tile)
+            product = jnp.dot(
+                hidden[block, group(crosses)], wdown[deep, span], preferred_element_type=F32
+            )
+            down_sum[:, span] = product if begin else down_sum[:, span] + product
+
+    for crosses, across, beside in (
+        (False, near_across, near_beside),
+        (True, cross_across, cross_beside),
+    ):
+
+        @pl.loop(1, chips)
+        def _(k):
+            across(k).wait_recv()
+            beside(k).start()
+
+        down(tp, crosses, True)
+        beside(0).wait_recv()
+        down(sibling, crosses, False)
+
+        @pl.loop(1, chips)
+        def _(k):
+            down(chip_behind(k), crosses, False)
+            beside(k).wait_recv()
+            down(chip_behind(k) + other - core, crosses, False)
+
+        result[members(crosses)] = down_sum[...].reshape(near, slots, wide).astype(BF16)
+
+        @pl.loop(near if crosses else 1, experts if crosses else near)
+        def _(j):
+            give_back(j, crosses).start()
+
+        if not crosses:
+            own = pltpu.make_async_copy(result.at[me], returned.at[me], self_sem.at[1])
+            own.start()
 
     @pl.loop(1, chips)
     def _(k):
@@ -300,43 +429,6 @@
             normed = blocks[b] * scale * gain_ref[:, lanes] + shift_ref[:, lanes]
             swished[b, span, :] = jax.nn.silu(normed).astype(BF16)
 
-    loads[6].wait()
-    wide = down_sum.shape[1]
-    tile, steps = tiles(wide, 256)
-
-    def down(block, begin):
-        deep = pl.ds(pl.multiple_of(block * units, units), units)
-
-        @pl.loop(0, steps)
-        def _(i):
-            span = pl.ds(pl.multiple_of(i * tile, tile), tile)
-            product = jnp.dot(hidden[block], wdown[deep, span], preferred_element_type=F32)
-            down_sum[:, span] = product if begin else down_sum[:, span] + product
-
-    down(tp, True)
-    hid_beside(0).wait_recv()
-    down(sibling, False)
-
-    @pl.loop(1, chips)
-    def _(k):
-        hid_across(k).wait_recv()
-        hid_beside(k).start()
-        down(chip_behind(k), False)
-        hid_beside(k).wait_recv()
-        down(chip_behind(k) + other - core, False)
-
-    result[...] = down_sum[...].reshape(experts, slots, wide).astype(BF16)
-
-    def give_back(k):
-        return remote(result.at[ahead(k)], returned.at[me], ret_send.at[k], ret_recv.at[k], ep=ahead(k))
-
-    @pl.loop(1, experts)
-    def _(k):
-        give_back(k).start()
-
-    own = pltpu.make_async_copy(result.at[me], returned.at[me], self_sem.at[1])
-    own.start()
-
     loads[5].wait()
     tile, steps = tiles(mixer.shape[1], 256)
 
@@ -368,9 +460,11 @@
 
     own.wait()
 
-    @pl.loop(1, experts)
-    def _(k):
-        give_back(k).wait_recv()
+    for crosses in (False, True):
+
+        @pl.loop(near if crosses else 1, experts if crosses else near)
+        def _(j):
+            give_back(j, crosses).wait_recv()
 
     tile, steps = tiles(wide, 512)
     for i in range(steps):
@@ -388,24 +482,36 @@
     put_expert = pltpu.make_async_copy(combined, expert_hbm, out_sem.at[1])
     put_expert.start()
 
-    @pl.loop(1, experts)
-    def _(k):
-        dispatch(k).wait_send()
-        give_back(k).wait_send()
-
-    @pl.loop(0, experts)
-    def _(k):
-        forward(k, send_rows.at[me]).wait_send()
-
-    @pl.loop(1, chips)
-    def _(k):
-        conv_across(k).wait_send()
-        hid_across(k).wait_send()
-
-    @pl.loop(0, chips)
-    def _(k):
-        conv_beside(k).wait_send()
-        hid_beside(k).wait_send()
+    for crosses in (False, True):
+
+        @pl.loop(near if crosses else 1, experts if crosses else near)
+        def _(j):
+            dispatch(j, crosses).wait_send()
+            give_back(j, crosses).wait_send()
+
+        @pl.loop(near if crosses else 0, experts if crosses else near)
+        def _(j):
+            @pl.loop(1, chips)
+            def _(k):
+                to_far(j, k, crosses).wait_send()
+
+            @pl.loop(0, chips)
+            def _(k):
+                to_side(j, k, crosses).wait_send()
+
+    for across, beside in (
+        (conv_across, conv_beside),
+        (near_across, near_beside),
+        (cross_across, cross_beside),
+    ):
+
+        @pl.loop(1, chips)
+        def _(k):
+            across(k).wait_send()
+
+        @pl.loop(0, chips)
+        def _(k):
+            beside(k).wait_send()
 
     put_mixer.wait()
     put_expert.wait()
@@ -432,7 +538,7 @@
     count, model = expert_input.shape
     slots = 2 * count // experts
     rows = experts * slots
-    half = model // CORES
+    part_width = model // parts
     units, wide = expert_gate.shape[2], expert_down.shape[2]
     out_width = out_weight.shape[1]
     chips = parts // CORES
@@ -451,17 +557,15 @@
         scratch_shapes=[
             pltpu.VMEM((channels, length), BF16),
             pltpu.VMEM((channels, length), BF16),
-            pltpu.VMEM((count, half), BF16),
+            pltpu.VMEM((count, part_width), BF16),
             pltpu.VMEM((model, units), BF16),
             pltpu.VMEM((model, units), BF16),
             pltpu.VMEM(expert_down.shape[1:], BF16),
             pltpu.VMEM(out_weight.shape, BF16),
-            pltpu.VMEM((experts, slots, half), BF16),
-            pltpu.VMEM((CORES, experts, slots, half), BF16),
-            pltpu.VMEM((rows, units), F32),
-            pltpu.VMEM((rows, units), F32),
-            pltpu.VMEM((parts, rows, units), BF16),
-            pltpu.VMEM((rows, wide), F32),
+            pltpu.VMEM((experts, slots, part_width), BF16),
+            pltpu.VMEM((parts, experts, slots, part_width), BF16),
+            pltpu.VMEM((parts, 2, rows // 2, units), BF16),
+            pltpu.VMEM((rows // 2, wide), F32),
             pltpu.VMEM((experts, slots, wide), BF16),
             pltpu.VMEM((experts, slots, wide), BF16),
             pltpu.VMEM((length + 2 * edge, channels), F32),
@@ -476,14 +580,16 @@
             dma((2,)),
             dma((experts,)),
             dma((experts,)),
-            dma((experts,)),
-            dma((experts,)),
+            dma((chips * experts,)),
+            dma((chips * experts,)),
+            dma((chips * experts,)),
+            dma((chips * experts,)),
             dma((2,)),
             dma((2,)),
             dma((2 * chips,)),
             dma((2 * chips,)),
-            dma((2 * chips,)),
-            dma((2 * chips,)),
+            dma((2, 2 * chips)),
+            dma((2, 2 * chips)),
             dma((experts,)),
             dma((experts,)),
         ],

time: 61.3 us -> 63.3 us (1.033)
  the two profiles are of different devices: /device:TPU:11 before, /device:TPU:0 now
where the time goes in v2:
time: 63.3 us; the launch traced here: 63.1 us
  Pallas kernels  58.5 us (92%)
  local copies, waits for them, and re-layouts  3.93 us (6%)
  between operations  0.64 us (1%)
    pallas_call x1, Pallas kernels, local(): pl.pallas_call(functools.partial(kernel, experts, parts), out_shape=(jax....  58.5 us
    unnamed x2, local copies, waits for them, and re-layouts  3.93 us

profile of v2, /device:TPU:0, one launch (start us, length us, event | category | flops | bytes accessed | tf_op | source)
XLA Modules:
  0.0 63.1 jit_solution(3114801999740790345)
XLA Ops:
  0.6 58.5 %block.1 = (bf16[512,1024]{1,0:T(8,128)(2,1)}, bf16[128,1024]{1,0:T(8,128)(2,1)}) custom-call(bf16[256,512]{1,0:T(8,128)(2,1)} %value_hbm.1, bf16[256,512]{1,0:T(8,128)(2,1)} %gate_hbm.1, bf16[128,4096]{1,0:T(8,128)(2,1)} %input_hbm.1, bf16[1,4096,512]{2,1,0:T(8,128)(2,1)} %wgate_hbm.1, bf16[1,4096,512]{2,1,0:T(8,128)(2,1)} %wup_hbm.1, ...), custom_call_target="tpu_custom_call" | custom-call | tf_op jit(solution)/shard_map/block/pallas_call | solution.py:549
  59.2 2.3 %copy.17 = bf16[512,1024]{1,0:T(8,128)(2,1)} copy(bf16[512,1024]{1,0:T(8,128)(2,1)} %get-tuple-element.4) | data formatting | bytes 2097152
  61.4 1.7 %copy.18 = bf16[128,1024]{1,0:T(8,128)(2,1)} copy(bf16[128,1024]{1,0:T(8,128)(2,1)} %get-tuple-element.5) | data formatting | bytes 524288
